TPU v7x, 32 devices: a whole 2x2x4 slice. The times are simulated.
32 devices in a mesh: ep: 8 (over z, core), tp: 4 (over y, x).
Axes of the slice: x: 2, y: 2, z: 4, core: 2. Of those that a mesh axis runs over, the one named last changes fastest.
Arguments:
- mixer_rows: bfloat16 [4096, 2048], P('ep', 'tp'), may hold values from -6 to 6
- expert_rows: bfloat16 [4096, 2048], P('ep', 'tp'), may hold values from -6 to 6
- mixer_gain: float32 [2048], replicated, may hold values from 0.1 to 1.9
- pool_scale: float32 [2048], P('tp'), may hold values from 0.1 to 1.9
- w_in: bfloat16 [2048, 2048], P(None, 'tp'), may hold values from -0.125 to 0.125
- w_mix_out: bfloat16 [2048, 2048], P(None, 'tp'), may hold values from -0.125 to 0.125
- expert_gain: float32 [2048], replicated, may hold values from 0.1 to 1.9
- expert_gate: bfloat16 [8, 2048, 2048], P('ep', None, 'tp'), may hold values from -0.125 to 0.125
- expert_up: bfloat16 [8, 2048, 2048], P('ep', None, 'tp'), may hold values from -0.125 to 0.125
- expert_down: bfloat16 [8, 2048, 2048], P('ep', None, 'tp'), may hold values from -0.125 to 0.125
- routes: int32 [4096, 2], P('ep'), may hold values from 0 to 7, all different within a row; in each aligned block of 512 rows (0 to 511, 512 to 1023, ...) at most 192 rows name the same one
- route_weight: float32 [4096, 2], P('ep'), may hold values from 0.1 to 1
Outputs:
- mixer_output: bfloat16 [4096, 2048], P('ep', 'tp')
- expert_output: bfloat16 [4096, 2048], P('ep', 'tp')
Inputs may be any that keep to these rules, and one draw needn't show every extreme that they name: `routes`: each row names 2 different experts. Among the rows of one device (aligned blocks of 512 rows) no expert is named more than 192 times, a bound that some block reaches.
All inputs are finite; a program needn't handle non-finite values.
Results may differ from a plain program's by a relative error of at most 0.0071.
Values may be sent and summed in bfloat16 or wider, within the bound.
No kernel may reach another device: no remote copies, remote signals or barrier semaphores. Data moves between devices by JAX's collectives and lax.ppermute only.
A program may use at most 64 MiB of HBM per device.

v0:
```python
import jax
import jax.numpy as jnp
from jax import lax
from jax.sharding import PartitionSpec as P

PW = 2048
TOP = 2
norm_eps = 1e-05
pool_windows = (2, 4, 8, 16)
rim_rows = 8


def extended_2(block, sides, width):
    for axis, dim in sides:
        count = lax.axis_size(axis)
        forward = [(i, i + 1) for i in range(count - 1)]
        backward = [(target, source) for source, target in forward]
        low = lax.ppermute(
            lax.slice_in_dim(block, block.shape[dim] - width, None, axis=dim), axis, forward
        )
        high = lax.ppermute(lax.slice_in_dim(block, 0, width, axis=dim), axis, backward)
        block = jnp.concatenate([low, block, high], axis=dim)
    return block


def layer_norm(row_block, gain_vec):
    values = row_block.astype(jnp.float32)
    center = values - jnp.mean(values, axis=-1, keepdims=True)
    spread = jnp.mean(center * center, axis=-1, keepdims=True)
    return (center * lax.rsqrt(spread + norm_eps) * gain_vec).astype(jnp.bfloat16)


def pooled_channels(inner_t, scale_local, ep_size, ep_index, tp_index):
    extended = extended_2(inner_t, (("ep", 1),), rim_rows).astype(jnp.float32)
    values = inner_t.astype(jnp.float32)
    channels = values.shape[0]
    row_count = values.shape[1]
    seq_len = row_count * ep_size
    position = ep_index * row_count + jnp.arange(row_count, dtype=jnp.int32)
    channel = tp_index * channels + jnp.arange(channels, dtype=jnp.int32)
    group = channel // (PW // 4)
    running = jnp.zeros((channels, row_count), jnp.float32)
    result = jnp.zeros((channels, row_count), jnp.float32)
    last_half = 0
    for group_id, window in enumerate(pool_windows):
        half_span = window // 2
        for offset in list(range(-half_span, -last_half)) + list(range(last_half, half_span)):
            running = running + extended[:, rim_rows + offset : rim_rows + offset + row_count]
        last_half = half_span
        lower_end = jnp.clip(position - half_span, 0, seq_len)
        upper_end = jnp.clip(position - half_span + window, 0, seq_len)
        counts = (upper_end - lower_end).astype(jnp.float32)
        member = (group == group_id)[:, None]
        result = jnp.where(member, running / counts[None, :], result)
    return ((result - values) * scale_local[:, None]).astype(jnp.bfloat16)


def on_device(
    mixer_rows,
    expert_rows,
    mixer_gain,
    pool_scale,
    w_in,
    w_mix_out,
    expert_gain,
    expert_gate,
    expert_up,
    expert_down,
    routes,
    route_weight,
):
    ep_size = lax.axis_size("ep")
    ep_index = lax.axis_index("ep")
    tp_index = lax.axis_index("tp")
    row_count = routes.shape[0]
    capacity = (3 * TOP * row_count + 2 * ep_size - 1) // (2 * ep_size)
    flat_route = routes.reshape(-1)
    onehot = (flat_route[:, None] == jnp.arange(ep_size, dtype=jnp.int32)[None, :]).astype(
        jnp.int32
    )
    ranking = jnp.sum(onehot * (jnp.cumsum(onehot, axis=0) - 1), axis=1)
    target = flat_route * capacity + ranking
    sender = (
        jnp.zeros((ep_size * capacity,), jnp.int32)
        .at[target]
        .set(jnp.arange(row_count * TOP, dtype=jnp.int32) // TOP + 1)
    )
    filled = (sender > 0)[:, None]
    source_row = jnp.maximum(sender - 1, 0)
    full_mix = lax.all_gather(mixer_rows, "tp", axis=1, tiled=True)
    feature_count = expert_rows.shape[1]
    outgoing = jnp.where(filled, expert_rows[source_row], jnp.zeros((), jnp.bfloat16))
    arrived = lax.all_to_all(
        outgoing.reshape(ep_size, capacity, feature_count),
        "ep",
        split_axis=0,
        concat_axis=0,
        tiled=True,
    )
    slot_slices = arrived.reshape(ep_size * capacity, feature_count)
    slot_normed = layer_norm(lax.all_gather(slot_slices, "tp", axis=1, tiled=True), expert_gain)
    contract_first = (((0,), (1,)), ((), ()))
    normed_mix = layer_norm(full_mix, mixer_gain)
    inner_t = lax.dot_general(
        w_in, normed_mix, contract_first, preferred_element_type=jnp.float32
    ).astype(jnp.bfloat16)
    pooled_t = pooled_channels(inner_t, pool_scale, ep_size, ep_index, tp_index)
    gate_t = lax.dot_general(
        expert_gate[0], slot_normed, contract_first, preferred_element_type=jnp.float32
    )
    up_t = lax.dot_general(
        expert_up[0], slot_normed, contract_first, preferred_element_type=jnp.float32
    )
    hidden_t = (jax.nn.silu(gate_t) * up_t).astype(jnp.bfloat16)
    contract_lead = (((0,), (0,)), ((), ()))
    down_weight = expert_down[0]
    mixed_sum = lax.dot_general(
        lax.all_gather(pooled_t, "tp", axis=0, tiled=True),
        w_mix_out,
        contract_lead,
        preferred_element_type=jnp.float32,
    )
    expert_sum = lax.dot_general(
        lax.all_gather(hidden_t, "tp", axis=0, tiled=True),
        down_weight,
        contract_lead,
        preferred_element_type=jnp.float32,
    )
    mixer_output = mixed_sum.astype(jnp.bfloat16)
    back_rows = expert_sum.astype(jnp.bfloat16).reshape(ep_size, capacity, expert_sum.shape[1])
    returned = lax.all_to_all(back_rows, "ep", split_axis=0, concat_axis=0, tiled=True).reshape(
        ep_size * capacity, expert_sum.shape[1]
    )
    picked = returned[target].astype(jnp.float32).reshape(row_count, TOP, expert_sum.shape[1])
    expert_output = jnp.sum(picked * route_weight[:, :, None], axis=1).astype(jnp.bfloat16)
    return (mixer_output, expert_output)


def solution(mesh):
    return jax.shard_map(
        on_device,
        mesh=mesh,
        in_specs=(
            P("ep", "tp"),
            P("ep", "tp"),
            P(),
            P("tp"),
            P(None, "tp"),
            P(None, "tp"),
            P(),
            P("ep", None, "tp"),
            P("ep", None, "tp"),
            P("ep", None, "tp"),
            P("ep", None),
            P("ep", None),
        ),
        out_specs=(P("ep", "tp"), P("ep", "tp")),
        check_vma=False,
    )
```

profile of v0, /device:TPU:0, one launch (start us, length us, event | category | flops | bytes accessed | tf_op | source)
XLA Modules:
  0.0 316.2 jit_solution(4581051959690600166)
XLA Ops:
  7.2 0.0 copy-start
  7.2 0.0 copy-start.1
  7.2 0.0 all-gather.9.cloned.1.call-start
  7.2 1.0 copy.16
  8.2 0.2 eq.66
  8.4 0.2 eq.62
  8.6 0.7 broadcast_multiply_fusion.1
  9.3 2.3 reduce-window.6
  11.6 0.3 slice_reduce_fusion
  11.8 0.2 reduce-window.9
  12.0 0.1 add_bitcast_fusion
  12.1 0.2 copy.15
  12.2 0.2 mul.97
  12.5 4.3 %scatter_custom_fusion = s32[1536]{0:T(1024)S(1)} fusion(s32[1024]{0:T(1024)S(1)} %bitcast.50, s32[1024]{0:T(1024)S(1)} %fusion.34, s32[]{:T(128)} %constant.78.clone.1), kind=kCustom, calls=%fused_computation.76 | custom fusion | bytes 6148 | tf_op jit(solution)/shard_map/scatter | solution.py:86
  16.8 0.1 broadcast_in_dim.68
  16.9 0.0 copy-done.1
  16.9 5.4 %gather_fusion = bf16[1536,512]{1,0:T(8,128)(2,1)} fusion(bf16[512,512]{1,0:T(8,128)(2,1)S(1)} %copy-done.1, s32[2048]{0:T(1024)S(1)} %pad_clamp_fusion), kind=kCustom, calls=%fused_computation | custom fusion | bytes 3151872 | tf_op jit(solution)/shard_map/gather | solution.py:92
  22.3 1.7 broadcast_select_fusion
  24.0 44.1 %all_to_all.10 = bf16[8,192,512]{2,1,0:T(8,128)(2,1)} all-to-all(bf16[8,192,512]{2,1,0:T(8,128)(2,1)S(1)} %broadcast_select_fusion), channel_id=1, replica_groups=mesh['ep'=8,'tp'=4] {'ep'}, dimensions={0} | all-to-all | bytes 3145728 | tf_op jit(solution)/shard_map/all_to_all | solution.py:93
  68.1 0.0 all-gather.9.cloned.1.call-update
  68.1 0.0 all-gather.5.cloned.1.call-start
  68.2 0.7 all-gather.5.cloned.1.call-update
  68.9 0.0 all-gather.11.cloned.1.call-start
  68.9 68.2 %all-gather.9.cloned.1.call-done = bf16[1536,2048]{1,0:T(8,128)(2,1)} async-done(((bf16[1536,512]{1,0:T(8,128)(2,1)}), bf16[1536,2048]{1,0:T(8,128)(2,1)}) %all-gather.9.cloned.1.call-update) | async-done | bytes 6291472 | tf_op jit(solution)/shard_map/all_gather | solution.py:101
  137.1 0.0 copy-start.2
  137.1 3.8 %convert_reduce_fusion = f32[1536]{0:T(1024)S(1)} fusion(bf16[1536,2048]{1,0:T(8,128)(2,1)} %all-gather.9.cloned.1.call-done), kind=kLoop, calls=%fused_computation.4 | loop fusion | flops 6289920 | bytes 6297600 | tf_op jit(solution)/shard_map/reduce_sum | solution.py:28
  140.9 0.8 copy-done.2
  141.7 1.8 fusion.2
  143.5 0.0 copy-done.4
  143.5 2.4 fusion.4
  145.9 0.0 copy-done
  145.9 0.0 copy-start.7
  146.0 3.4 %convolution_bitcast_fusion.1 = f32[512,1536]{0,1:T(8,128)S(1)} fusion(bf16[1536,2048]{1,0:T(8,128)(2,1)S(1)} %fusion.4, bf16[1,2048,512]{2,1,0:T(8,128)(2,1)S(1)} %copy-done), kind=kOutput, calls=%fused_computation.19 | convolution fusion | flops 3221225472 | bytes 11534336 | tf_op jit(solution)/shard_map/dot_general | solution.py:108
  149.4 0.0 copy-done.7
  149.4 4.8 %fusion.11 = bf16[512,1536]{0,1:T(8,128)(2,1)} fusion(bf16[1536,2048]{1,0:T(8,128)(2,1)S(1)} %fusion.4, f32[512,1536]{0,1:T(8,128)S(1)} %convolution_bitcast_fusion.1, bf16[1,2048,512]{2,1,0:T(8,128)(2,1)S(1)} %copy-done.7), kind=kOutput, calls=%fused_computation.20 | convolution fusion | flops 3225944064 | bytes 13107200 | tf_op jit(solution)/shard_map/dot_general | solution.py:111
  154.2 0.0 all-gather.11.cloned.1.call-update
  154.3 0.2 all-gather.7.cloned.1.call-start
  154.5 19.4 %all-gather.5.cloned.1.call-done = bf16[512,2048]{1,0:T(8,128)(2,1)} async-done(((bf16[512,512]{1,0:T(8,128)(2,1)}), bf16[512,2048]{1,0:T(8,128)(2,1)}) %all-gather.5.cloned.1.call-update) | async-done | bytes 2097168 | tf_op jit(solution)/shard_map/all_gather | solution.py:90
  174.0 2.1 convert_reduce_fusion.1
  176.1 0.1 copy-done.3
  176.2 0.7 fusion.7
  176.9 0.0 copy-done.8
  176.9 0.0 copy-done.9
  176.9 0.0 copy-start.6
  176.9 1.3 fusion.23
  178.3 1.6 collective-permute-start
  179.9 1.3 collective-permute-start.1
  181.2 0.0 collective-permute-done
  181.2 3.2 %collective-permute-done.1 = bf16[512,8]{0,1:T(8,128)(2,1)S(1)} collective-permute-done((bf16[512,8]{0,1:T(8,128)(2,1)S(1)}, bf16[512,8]{0,1:T(8,128)(2,1)S(1)}, u32[]{:S(2)}, u32[]{:S(2)}) %collective-permute-start.1) | collective-permute-done | bytes 8224 | tf_op jit(solution)/shard_map/ppermute | solution.py:21
  184.4 0.1 maximum_convert_fusion
  184.5 0.0 copy-done.6
  184.5 3.3 %fusion.30 = bf16[512,512]{0,1:T(8,128)(2,1)} fusion(bf16[512,512]{0,1:T(8,128)(2,1)S(1)} %fusion.23, f32[512,528]{0,1:T(8,128)S(1)} %maximum_convert_fusion, f32[512]{0:T(512)S(1)} %copy-done.6, f32[512]{0:T(512)S(1)} %get-tuple-element.4, f32[512]{0:T(512)S(1)} %get-tuple-element.5, f32[512]{0:T(512)S(1)} %get-tuple-element.6, ...), kind=kLoop, calls=%fused_computation.53 | loop fusion | flops 7077888 | bytes 17838080 | tf_op jit(solution)/shard_map/convert_element_type | solution.py:55
  187.8 0.0 all-gather.7.cloned.1.call-update
  187.8 57.9 %all-gather.11.cloned.1.call-done = bf16[2048,1536]{0,1:T(8,128)(2,1)} async-done(((bf16[512,1536]{0,1:T(8,128)(2,1)}), bf16[2048,1536]{0,1:T(8,128)(2,1)}) %all-gather.11.cloned.1.call-update) | async-done | bytes 6291472 | tf_op jit(solution)/shard_map/all_gather | solution.py:124
  245.8 8.1 %convolution_convert_fusion = bf16[1536,512]{1,0:T(8,128)(2,1)} fusion(bf16[2048,1536]{0,1:T(8,128)(2,1)} %all-gather.11.cloned.1.call-done, bf16[1,2048,512]{2,1,0:T(8,128)(2,1)} %param.21), kind=kOutput, calls=%fused_computation.21 | convolution fusion | flops 3222011904 | bytes 9961472 | tf_op jit(solution)/shard_map/dot_general | solution.py:123
  253.8 4.7 %all-to-all-start.1 = ((bf16[8,192,512]{2,1,0:T(8,128)(2,1)}), bf16[8,192,512]{2,1,0:T(8,128)(2,1)}, u32[]{:S(2)}, u32[]{:S(2)}) async-start(bf16[8,192,512]{2,1,0:T(8,128)(2,1)} %bitcast.48), calls=%async_computation.1 | async-start | bytes 3145728 | tf_op jit(solution)/shard_map/all_to_all | solution.py:131
  258.6 0.0 copy-done.5
  258.6 0.1 copy.18
  258.7 24.3 %all-gather.7.cloned.1.call-done = bf16[2048,512]{0,1:T(8,128)(2,1)} async-done(((bf16[512,512]{0,1:T(8,128)(2,1)}), bf16[2048,512]{0,1:T(8,128)(2,1)}) %all-gather.7.cloned.1.call-update) | async-done | bytes 2097168 | tf_op jit(solution)/shard_map/all_gather | solution.py:118
  283.1 4.3 %convolution_convert_fusion.1 = bf16[512,512]{1,0:T(8,128)(2,1)} fusion(bf16[2048,512]{0,1:T(8,128)(2,1)} %all-gather.7.cloned.1.call-done, bf16[2048,512]{1,0:T(8,128)(2,1)} %param.17), kind=kOutput, calls=%fused_computation.32 | convolution fusion | flops 1074003968 | bytes 4718592 | tf_op jit(solution)/shard_map/dot_general | solution.py:117
  287.4 9.1 %all-to-all-done.1 = bf16[8,192,512]{2,1,0:T(8,128)(2,1)} async-done(((bf16[8,192,512]{2,1,0:T(8,128)(2,1)}), bf16[8,192,512]{2,1,0:T(8,128)(2,1)}, u32[]{:S(2)}, u32[]{:S(2)}) %all-to-all-start.1) | async-done | bytes 1572896 | tf_op jit(solution)/shard_map/all_to_all | solution.py:131
  296.5 5.6 %gather_fusion.1 = bf16[1024,512]{1,0:T(8,128)(2,1)S(1)} fusion(bf16[1536,512]{1,0:T(8,128)(2,1)} %bitcast.12, s32[1024]{0:T(1024)S(1)} %broadcast_clamp_fusion), kind=kCustom, calls=%fused_computation.1 | custom fusion | bytes 2101248 | tf_op jit(solution)/shard_map/gather | solution.py:134
  302.1 2.4 reshape.168
  304.4 5.2 %multiply_reduce_fusion = bf16[512,512]{1,0:T(8,128)(2,1)} fusion(f32[512,2,512]{2,1,0:T(2,128)} %reshape.168, f32[512,2]{1,0:T(8,128)S(1)} %copy.18), kind=kLoop, calls=%fused_computation.26 | loop fusion | flops 786432 | bytes 2625536 | tf_op jit(solution)/shard_map/reduce_sum | solution.py:135
  (22 shorter events, 0.1 us)
Async XLA Ops:
  7.2 138.8 %copy-start = (bf16[1,2048,512]{2,1,0:T(8,128)(2,1)S(1)}, bf16[1,2048,512]{2,1,0:T(8,128)(2,1)}, u32[]{:S(2)}) copy-start(bf16[1,2048,512]{2,1,0:T(8,128)(2,1)} %param.19) | copy-start | bytes 6291460
  7.2 9.8 %copy-start.1 = (bf16[512,512]{1,0:T(8,128)(2,1)S(1)}, bf16[512,512]{1,0:T(8,128)(2,1)}, u32[]{:S(2)}) copy-start(bf16[512,512]{1,0:T(8,128)(2,1)} %param.13) | copy-start | bytes 1572868
  7.2 129.9 %all-gather.9.cloned.1.call-start = ((), (), s32[]{:S(2)}) async-start(), calls=%async_computation.4 | async-start | bytes 7864320 | tf_op jit(solution)/shard_map/all_gather | solution.py:101
  68.1 105.9 %all-gather.5.cloned.1.call-start = ((), (), s32[]{:S(2)}) async-start(), calls=%async_computation.2 | async-start | bytes 2621440 | tf_op jit(solution)/shard_map/all_gather | solution.py:90
  68.9 176.9 %all-gather.11.cloned.1.call-start = ((), (), s32[]{:S(2)}) async-start(), calls=%async_computation.5 | async-start | bytes 7864320 | tf_op jit(solution)/shard_map/all_gather | solution.py:124
  137.1 4.6 %copy-start.2 = (bf16[1536,2048]{1,0:T(8,128)(2,1)S(1)}, bf16[1536,2048]{1,0:T(8,128)(2,1)}, u32[]{:S(2)}) copy-start(bf16[1536,2048]{1,0:T(8,128)(2,1)} %all-gather.9.cloned.1.call-done) | copy-start | bytes 18874372
  141.7 1.8 copy-start.4
  145.9 3.5 %copy-start.7 = (bf16[1,2048,512]{2,1,0:T(8,128)(2,1)S(1)}, bf16[1,2048,512]{2,1,0:T(8,128)(2,1)}, u32[]{:S(2)}) copy-start(bf16[1,2048,512]{2,1,0:T(8,128)(2,1)} %param.20) | copy-start | bytes 6291460
  154.3 128.8 %all-gather.7.cloned.1.call-start = ((), (), s32[]{:S(2)}) async-start(), calls=%async_computation.3 | async-start | bytes 2621440 | tf_op jit(solution)/shard_map/all_gather | solution.py:118
  174.0 2.2 copy-start.3
  174.0 2.9 copy-start.8
  174.0 2.9 copy-start.9
  176.9 7.6 %copy-start.6 = (f32[512]{0:T(512)S(1)}, f32[512]{0:T(512)}, u32[]{:S(2)}) copy-start(f32[512]{0:T(512)} %param.15) | copy-start | bytes 6148
  178.3 2.9 collective-permute-start
  179.9 4.5 %collective-permute-start.1 = (bf16[512,8]{0,1:T(8,128)(2,1)S(1)}, bf16[512,8]{0,1:T(8,128)(2,1)S(1)}, u32[]{:S(2)}, u32[]{:S(2)}) collective-permute-start(bf16[512,8]{0,1:T(8,128)(2,1)S(1)} %get-tuple-element.3), channel_id=1, source_target_pairs={{4,0},{8,4},{12,8},{16,12},{20,16},{24,20},{28,24},{5,1},{9,5},{13... | collective-permute-start | bytes 24584 | tf_op jit(solution)/shard_map/ppermute | solution.py:21
  253.8 4.7 %copy-start.5 = (f32[512,2]{0,1:T(2,128)S(1)}, f32[512,2]{0,1:T(2,128)}, u32[]{:S(2)}) copy-start(f32[512,2]{0,1:T(2,128)} %param.23) | copy-start | bytes 12292
  253.8 42.6 %all-to-all-start.1 = ((bf16[8,192,512]{2,1,0:T(8,128)(2,1)}), bf16[8,192,512]{2,1,0:T(8,128)(2,1)}, u32[]{:S(2)}, u32[]{:S(2)}) async-start(bf16[8,192,512]{2,1,0:T(8,128)(2,1)} %bitcast.48), calls=%async_computation.1 | async-start | bytes 3145728 | tf_op jit(solution)/shard_map/all_to_all | solution.py:131
Sparse Core Ops, SparseCore 0:
  68.2 68.8 all-gather.8
  138.9 35.0 all-gather.4
  175.8 69.8 all-gather.10
  248.0 35.0 all-gather.6
where the time goes:
time: 317 us; the launch traced here: 316 us
  waiting for transfers between devices  183 us (58%)
  blocking collectives  44.1 us (14%)
  other arithmetic  24.5 us (8%)
  matrix products  21.9 us (7%)
  local copies, waits for them, and re-layouts  20.8 us (7%)
  between operations  14.1 us (4%)
  starting transfers between devices  7.95 us (3%)
    all_gather x1, waiting for transfers between devices, on_device(): lax.all_gather(slot_slices, 'tp', axis=1, tiled=True)  68.2 us
    all_gather x1, waiting for transfers between devices, on_device(): lax.all_gather(hidden_t, 'tp', axis=0, tiled=True)  57.9 us
    all_to_all x1, blocking collectives, on_device(): lax.all_to_all(outgoing.reshape(ep_size, capacity, feature_count), 'ep',...  44.1 us
    all_gather x1, waiting for transfers between devices, on_device(): lax.all_gather(pooled_t, 'tp', axis=0, tiled=True)  24.3 us
    all_gather x1, waiting for transfers between devices, on_device(): full_mix = lax.all_gather(mixer_rows, 'tp', axis=1, tiled=True)  19.4 us
    all_to_all x1, waiting for transfers between devices, on_device(): lax.all_to_all(back_rows, 'ep', split_axis=0, concat_axis=0, tiled=True)  9.13 us
    dot_general x1, matrix products, on_device(): lax.dot_general(lax.all_gather(hidden_t, 'tp', axis=0, tiled=True), down_...  8.08 us
  transfers between devices with their start and end apart: 7, of which 6 were waited for; matrix products, arithmetic and copies ran while one was open for 12% of the time, Pallas kernels for 0%

commit v1 on v0

--- a/solution.py
+++ b/solution.py
@@ -87,7 +87,12 @@
     )
     filled = (sender > 0)[:, None]
     source_row = jnp.maximum(sender - 1, 0)
-    full_mix = lax.all_gather(mixer_rows, "tp", axis=1, tiled=True)
+    ring = [mixer_rows]
+    for hop in range(3):
+        ring.append(lax.ppermute(ring[-1], "tp", [(dev, (dev + 1) % 4) for dev in range(4)]))
+    full_mix = jnp.roll(
+        jnp.concatenate(ring[::-1], axis=1), (lax.axis_index("tp") + 1) * ring[0].shape[1], axis=1
+    )
     feature_count = expert_rows.shape[1]
     outgoing = jnp.where(filled, expert_rows[source_row], jnp.zeros((), jnp.bfloat16))
     arrived = lax.all_to_all(

time: 317 us -> 314 us (level)
  waiting for transfers between devices: 183 us -> 174 us
  local copies, waits for them, and re-layouts: 20.8 us -> 25.4 us
  starting transfers between devices: 7.95 us -> 11.5 us
    ppermute x0 -> x3, waiting for transfers between devices: none -> 57.3 us  [on_device(): lax.ppermute(ring[-1], 'tp', [(dev, (dev + 1) % 4) for dev in range(4)])]
    all_gather x1, waiting for transfers between devices: 57.9 us -> 10.4 us  [on_device(): lax.all_gather(hidden_t, 'tp', axis=0, tiled=True)]
    all_gather x1 -> x0, waiting for transfers between devices: 19.4 us -> none  [on_device(): full_mix = lax.all_gather(mixer_rows, 'tp', axis=1, tiled=True)]
    unnamed x22 -> x29, local copies, waits for them, and re-layouts: 2.07 us -> 6.66 us
    ppermute x0 -> x3, starting transfers between devices: none -> 4.17 us  [on_device(): lax.ppermute(ring[-1], 'tp', [(dev, (dev + 1) % 4) for dev in range(4)])]
  transfers between devices with their start and end apart: 7 -> 9, of which waited for: 6 -> 8; matrix products, arithmetic and copies ran while one was open for 12% -> 7% of each run, Pallas kernels for 0% -> 0%
where the time goes in v1:
time: 314 us; the launch traced here: 313 us
  waiting for transfers between devices  174 us (55%)
  blocking collectives  44.1 us (14%)
  local copies, waits for them, and re-layouts  25.4 us (8%)
  other arithmetic  22.7 us (7%)
  matrix products  21.9 us (7%)
  between operations  14.1 us (4%)
  starting transfers between devices  11.5 us (4%)
    all_gather x1, waiting for transfers between devices, on_device(): lax.all_gather(slot_slices, 'tp', axis=1, tiled=True)  68.9 us
    ppermute x3, waiting for transfers between devices, on_device(): lax.ppermute(ring[-1], 'tp', [(dev, (dev + 1) % 4) for dev in range(4)])  57.3 us
    all_to_all x1, blocking collectives, on_device(): lax.all_to_all(outgoing.reshape(ep_size, capacity, feature_count), 'ep',...  44.1 us
    all_gather x1, waiting for transfers between devices, on_device(): lax.all_gather(pooled_t, 'tp', axis=0, tiled=True)  24.6 us
    all_gather x1, waiting for transfers between devices, on_device(): lax.all_gather(hidden_t, 'tp', axis=0, tiled=True)  10.4 us
    all_to_all x1, waiting for transfers between devices, on_device(): lax.all_to_all(back_rows, 'ep', split_axis=0, concat_axis=0, tiled=True)  8.83 us
    dot_general x1, matrix products, on_device(): lax.dot_general(lax.all_gather(hidden_t, 'tp', axis=0, tiled=True), down_...  8.08 us
    unnamed x29, local copies, waits for them, and re-layouts  6.66 us
  transfers between devices with their start and end apart: 9, of which 8 were waited for; matrix products, arithmetic and copies ran while one was open for 7% of the time, Pallas kernels for 0%

profile of v1, /device:TPU:0, one launch (start us, length us, event | category | flops | bytes accessed | tf_op | source)
XLA Modules:
  0.0 313.4 jit_solution(14929883607178266630)
XLA Ops:
  7.2 0.0 copy-start
  7.2 0.0 all-gather.6.cloned.1.call-start
  7.2 1.0 copy.16
  8.2 0.2 eq.69
  8.4 0.2 eq.65
  8.6 0.7 broadcast_multiply_fusion.1
  9.3 2.3 reduce-window.6
  11.6 0.3 slice_reduce_fusion
  11.8 0.2 reduce-window.9
  12.0 0.1 add_bitcast_fusion
  12.1 0.2 copy.15
  12.2 0.2 mul.101
  12.5 4.3 %scatter_custom_fusion = s32[1536]{0:T(1024)S(1)} fusion(s32[1024]{0:T(1024)S(1)} %bitcast.50, s32[1024]{0:T(1024)S(1)} %fusion.35, s32[]{:T(128)} %constant.97.clone.1), kind=kCustom, calls=%fused_computation.85 | custom fusion | bytes 6148 | tf_op jit(solution)/shard_map/scatter | solution.py:86
  16.8 0.1 broadcast_in_dim.68
  16.9 5.4 %gather_fusion = bf16[1536,512]{1,0:T(8,128)(2,1)} fusion(bf16[512,512]{1,0:T(8,128)(2,1)S(1)} %copy-done.1, s32[2048]{0:T(1024)S(1)} %pad_clamp_fusion), kind=kCustom, calls=%fused_computation | custom fusion | bytes 3151872 | tf_op jit(solution)/shard_map/gather | solution.py:97
  22.3 1.7 broadcast_select_fusion
  24.0 44.1 %all_to_all.10 = bf16[8,192,512]{2,1,0:T(8,128)(2,1)} all-to-all(bf16[8,192,512]{2,1,0:T(8,128)(2,1)S(1)} %broadcast_select_fusion), channel_id=1, replica_groups=mesh['ep'=8,'tp'=4] {'ep'}, dimensions={0} | all-to-all | bytes 3145728 | tf_op jit(solution)/shard_map/all_to_all | solution.py:98
  68.1 0.0 all-gather.6.cloned.1.call-update
  68.1 0.0 all-gather.8.cloned.1.call-start
  68.2 68.9 %all-gather.6.cloned.1.call-done = bf16[1536,2048]{1,0:T(8,128)(2,1)} async-done(((bf16[1536,512]{1,0:T(8,128)(2,1)}), bf16[1536,2048]{1,0:T(8,128)(2,1)}) %all-gather.6.cloned.1.call-update) | async-done | bytes 6291472 | tf_op jit(solution)/shard_map/all_gather | solution.py:106
  137.1 3.8 %convert_reduce_fusion = f32[1536]{0:T(1024)S(1)} fusion(bf16[1536,2048]{1,0:T(8,128)(2,1)} %all-gather.6.cloned.1.call-done), kind=kLoop, calls=%fused_computation.4 | loop fusion | flops 6289920 | bytes 6297600 | tf_op jit(solution)/shard_map/reduce_sum | solution.py:28
  140.9 0.8 copy-done.2
  141.7 1.8 fusion.2
  143.5 2.4 fusion.4
  145.9 0.0 copy-start.7
  146.0 3.4 %convolution_bitcast_fusion.1 = f32[512,1536]{0,1:T(8,128)S(1)} fusion(bf16[1536,2048]{1,0:T(8,128)(2,1)S(1)} %fusion.4, bf16[1,2048,512]{2,1,0:T(8,128)(2,1)S(1)} %copy-done), kind=kOutput, calls=%fused_computation.19 | convolution fusion | flops 3221225472 | bytes 11534336 | tf_op jit(solution)/shard_map/dot_general | solution.py:113
  149.4 0.0 copy-start.3
  149.4 4.8 %fusion.11 = bf16[512,1536]{0,1:T(8,128)(2,1)} fusion(bf16[1536,2048]{1,0:T(8,128)(2,1)S(1)} %fusion.4, f32[512,1536]{0,1:T(8,128)S(1)} %convolution_bitcast_fusion.1, bf16[1,2048,512]{2,1,0:T(8,128)(2,1)S(1)} %copy-done.7), kind=kOutput, calls=%fused_computation.20 | convolution fusion | flops 3225944064 | bytes 13107200 | tf_op jit(solution)/shard_map/dot_general | solution.py:116
  154.2 0.0 all-gather.8.cloned.1.call-update
  154.3 0.0 all-gather.4.cloned.1.call-start
  154.3 1.5 collective-permute-start
  155.8 16.7 %collective-permute-done = bf16[512,512]{1,0:T(8,128)(2,1)S(1)} collective-permute-done((bf16[512,512]{1,0:T(8,128)(2,1)S(1)}, bf16[512,512]{1,0:T(8,128)(2,1)S(1)}, u32[]{:S(2)}, u32[]{:S(2)}) %collective-permute-start) | collective-permute-done | bytes 524320 | tf_op jit(solution)/shard_map/ppermute | solution.py:92
  172.5 2.0 collective-permute-start.1
  174.5 22.4 %collective-permute-done.1 = bf16[512,512]{1,0:T(8,128)(2,1)} collective-permute-done((bf16[512,512]{1,0:T(8,128)(2,1)S(1)}, bf16[512,512]{1,0:T(8,128)(2,1)}, u32[]{:S(2)}, u32[]{:S(2)}) %collective-permute-start.1) | collective-permute-done | bytes 524320 | tf_op jit(solution)/shard_map/ppermute | solution.py:92
  197.0 0.6 collective-permute-start.2
  197.6 18.2 %collective-permute-done.2 = bf16[512,512]{1,0:T(8,128)(2,1)} collective-permute-done((bf16[512,512]{1,0:T(8,128)(2,1)}, bf16[512,512]{1,0:T(8,128)(2,1)}, u32[]{:S(2)}, u32[]{:S(2)}) %collective-permute-start.2) | collective-permute-done | bytes 524320 | tf_op jit(solution)/shard_map/ppermute | solution.py:92
  215.9 1.1 constant_dynamic-update-slice_fusion.7
  217.0 1.1 constant_dynamic-update-slice_fusion.6
  218.1 0.1 constant_dynamic-update-slice_fusion.5
  218.1 0.1 constant_dynamic-update-slice_fusion.4
  218.2 0.0 copy-start.8
  218.2 1.2 constant_dynamic-update-slice_fusion.3
  219.5 1.1 constant_dynamic-update-slice_fusion.2
  220.6 0.1 constant_dynamic-update-slice_fusion.1
  220.7 0.1 constant_dynamic-update-slice_fusion
  220.7 0.4 convert_reduce_fusion.1
  221.1 0.7 fusion.7
  221.8 1.3 fusion.24
  223.2 1.3 collective-permute-start.3
  224.5 1.3 collective-permute-start.4
  225.8 3.5 %collective-permute-done.4 = bf16[512,8]{0,1:T(8,128)(2,1)S(1)} collective-permute-done((bf16[512,8]{0,1:T(8,128)(2,1)S(1)}, bf16[512,8]{0,1:T(8,128)(2,1)S(1)}, u32[]{:S(2)}, u32[]{:S(2)}) %collective-permute-start.4) | collective-permute-done | bytes 8224 | tf_op jit(solution)/shard_map/ppermute | solution.py:21
  229.3 0.1 maximum_convert_fusion
  229.4 3.3 %fusion.31 = bf16[512,512]{0,1:T(8,128)(2,1)} fusion(bf16[512,512]{0,1:T(8,128)(2,1)S(1)} %fusion.24, f32[512,528]{0,1:T(8,128)S(1)} %maximum_convert_fusion, f32[512]{0:T(512)S(1)} %copy-done.6, f32[512]{0:T(512)S(1)} %get-tuple-element.4, f32[512]{0:T(512)S(1)} %get-tuple-element.5, f32[512]{0:T(512)S(1)} %get-tuple-element.6, ...), kind=kLoop, calls=%fused_computation.54 | loop fusion | flops 7077888 | bytes 17838080 | tf_op jit(solution)/shard_map/convert_element_type | solution.py:55
  232.7 0.0 all-gather.4.cloned.1.call-update
  232.7 10.4 %all-gather.8.cloned.1.call-done = bf16[2048,1536]{0,1:T(8,128)(2,1)} async-done(((bf16[512,1536]{0,1:T(8,128)(2,1)}), bf16[2048,1536]{0,1:T(8,128)(2,1)}) %all-gather.8.cloned.1.call-update) | async-done | bytes 6291472 | tf_op jit(solution)/shard_map/all_gather | solution.py:129
  243.1 8.1 %convolution_convert_fusion = bf16[1536,512]{1,0:T(8,128)(2,1)} fusion(bf16[2048,1536]{0,1:T(8,128)(2,1)} %all-gather.8.cloned.1.call-done, bf16[1,2048,512]{2,1,0:T(8,128)(2,1)} %param.21), kind=kOutput, calls=%fused_computation.21 | convolution fusion | flops 3222011904 | bytes 9961472 | tf_op jit(solution)/shard_map/dot_general | solution.py:128
  251.2 4.6 %all-to-all-start.1 = ((bf16[8,192,512]{2,1,0:T(8,128)(2,1)}), bf16[8,192,512]{2,1,0:T(8,128)(2,1)}, u32[]{:S(2)}, u32[]{:S(2)}) async-start(bf16[8,192,512]{2,1,0:T(8,128)(2,1)} %bitcast.48), calls=%async_computation.1 | async-start | bytes 3145728 | tf_op jit(solution)/shard_map/all_to_all | solution.py:136
  255.8 0.1 copy.18
  256.0 24.6 %all-gather.4.cloned.1.call-done = bf16[2048,512]{0,1:T(8,128)(2,1)} async-done(((bf16[512,512]{0,1:T(8,128)(2,1)}), bf16[2048,512]{0,1:T(8,128)(2,1)}) %all-gather.4.cloned.1.call-update) | async-done | bytes 2097168 | tf_op jit(solution)/shard_map/all_gather | solution.py:123
  280.6 4.3 %convolution_convert_fusion.1 = bf16[512,512]{1,0:T(8,128)(2,1)} fusion(bf16[2048,512]{0,1:T(8,128)(2,1)} %all-gather.4.cloned.1.call-done, bf16[2048,512]{1,0:T(8,128)(2,1)} %param.17), kind=kOutput, calls=%fused_computation.33 | convolution fusion | flops 1074003968 | bytes 4718592 | tf_op jit(solution)/shard_map/dot_general | solution.py:122
  284.9 8.8 %all-to-all-done.1 = bf16[8,192,512]{2,1,0:T(8,128)(2,1)} async-done(((bf16[8,192,512]{2,1,0:T(8,128)(2,1)}), bf16[8,192,512]{2,1,0:T(8,128)(2,1)}, u32[]{:S(2)}, u32[]{:S(2)}) %all-to-all-start.1) | async-done | bytes 1572896 | tf_op jit(solution)/shard_map/all_to_all | solution.py:136
  293.7 5.6 %gather_fusion.1 = bf16[1024,512]{1,0:T(8,128)(2,1)S(1)} fusion(bf16[1536,512]{1,0:T(8,128)(2,1)} %bitcast.12, s32[1024]{0:T(1024)S(1)} %broadcast_clamp_fusion), kind=kCustom, calls=%fused_computation.1 | custom fusion | bytes 2101248 | tf_op jit(solution)/shard_map/gather | solution.py:139
  299.3 2.4 reshape.168
  301.7 5.2 %multiply_reduce_fusion = bf16[512,512]{1,0:T(8,128)(2,1)} fusion(f32[512,2,512]{2,1,0:T(2,128)} %reshape.168, f32[512,2]{1,0:T(8,128)S(1)} %copy.18), kind=kLoop, calls=%fused_computation.26 | loop fusion | flops 786432 | bytes 2625536 | tf_op jit(solution)/shard_map/reduce_sum | solution.py:140
  (33 shorter events, 0.2 us)
Async XLA Ops:
  7.2 138.8 %copy-start = (bf16[1,2048,512]{2,1,0:T(8,128)(2,1)S(1)}, bf16[1,2048,512]{2,1,0:T(8,128)(2,1)}, u32[]{:S(2)}) copy-start(bf16[1,2048,512]{2,1,0:T(8,128)(2,1)} %param.19) | copy-start | bytes 6291460
  7.2 9.8 %copy-start.1 = (bf16[512,512]{1,0:T(8,128)(2,1)S(1)}, bf16[512,512]{1,0:T(8,128)(2,1)}, u32[]{:S(2)}) copy-start(bf16[512,512]{1,0:T(8,128)(2,1)} %param.13) | copy-start | bytes 1572868
  7.2 129.9 %all-gather.6.cloned.1.call-start = ((), (), s32[]{:S(2)}) async-start(), calls=%async_computation.3 | async-start | bytes 7864320 | tf_op jit(solution)/shard_map/all_gather | solution.py:106
  68.1 175.0 %all-gather.8.cloned.1.call-start = ((), (), s32[]{:S(2)}) async-start(), calls=%async_computation.4 | async-start | bytes 7864320 | tf_op jit(solution)/shard_map/all_gather | solution.py:129
  137.1 4.6 %copy-start.2 = (bf16[1536,2048]{1,0:T(8,128)(2,1)S(1)}, bf16[1536,2048]{1,0:T(8,128)(2,1)}, u32[]{:S(2)}) copy-start(bf16[1536,2048]{1,0:T(8,128)(2,1)} %all-gather.6.cloned.1.call-done) | copy-start | bytes 18874372
  140.9 2.6 copy-start.4
  145.9 3.5 %copy-start.7 = (bf16[1,2048,512]{2,1,0:T(8,128)(2,1)S(1)}, bf16[1,2048,512]{2,1,0:T(8,128)(2,1)}, u32[]{:S(2)}) copy-start(bf16[1,2048,512]{2,1,0:T(8,128)(2,1)} %param.20) | copy-start | bytes 6291460
  149.4 4.9 %copy-start.3 = (bf16[512,512]{1,0:T(8,128)(2,1)S(1)}, bf16[512,512]{1,0:T(8,128)(2,1)}, u32[]{:S(2)}) copy-start(bf16[512,512]{1,0:T(8,128)(2,1)} %param.12) | copy-start | bytes 1572868
  154.3 126.3 %all-gather.4.cloned.1.call-start = ((), (), s32[]{:S(2)}) async-start(), calls=%async_computation.2 | async-start | bytes 2621440 | tf_op jit(solution)/shard_map/all_gather | solution.py:123
  154.3 18.2 %collective-permute-start = (bf16[512,512]{1,0:T(8,128)(2,1)S(1)}, bf16[512,512]{1,0:T(8,128)(2,1)S(1)}, u32[]{:S(2)}, u32[]{:S(2)}) collective-permute-start(bf16[512,512]{1,0:T(8,128)(2,1)S(1)} %copy-done.3), channel_id=1, source_target_pairs={{0,1},{1,2},{2,3},{3,0},{4,5},{5,6},{6,7},{7,4},{8,9},{9,10},{10,1... | collective-permute-start | bytes 1572872 | tf_op jit(solution)/shard_map/ppermute | solution.py:92
  172.5 24.5 %collective-permute-start.1 = (bf16[512,512]{1,0:T(8,128)(2,1)S(1)}, bf16[512,512]{1,0:T(8,128)(2,1)}, u32[]{:S(2)}, u32[]{:S(2)}) collective-permute-start(bf16[512,512]{1,0:T(8,128)(2,1)S(1)} %collective-permute-done), channel_id=1, source_target_pairs={{0,1},{1,2},{2,3},{3,0},{4,5},{5,6},{6,7},{7,4},{8,9},{9,10},{10,1... | collective-permute-start | bytes 1572872 | tf_op jit(solution)/shard_map/ppermute | solution.py:92
  197.0 18.9 %collective-permute-start.2 = (bf16[512,512]{1,0:T(8,128)(2,1)}, bf16[512,512]{1,0:T(8,128)(2,1)}, u32[]{:S(2)}, u32[]{:S(2)}) collective-permute-start(bf16[512,512]{1,0:T(8,128)(2,1)} %collective-permute-done.1), channel_id=1, source_target_pairs={{0,1},{1,2},{2,3},{3,0},{4,5},{5,6},{6,7},{7,4},{8,9},{9,10},{10,1... | collective-permute-start | bytes 1572872 | tf_op jit(solution)/shard_map/ppermute | solution.py:92
  218.2 3.6 %copy-start.8 = (bf16[2048,512]{1,0:T(8,128)(2,1)S(1)}, bf16[2048,512]{1,0:T(8,128)(2,1)}, u32[]{:S(2)}) copy-start(bf16[2048,512]{1,0:T(8,128)(2,1)} %param.16) | copy-start | bytes 6291460
  218.2 3.6 %copy-start.9 = (f32[2048]{0:T(1024)S(1)}, f32[2048]{0:T(1024)}, u32[]{:S(2)}) copy-start(f32[2048]{0:T(1024)} %param.14) | copy-start | bytes 24580
  221.8 7.6 %copy-start.6 = (f32[512]{0:T(512)S(1)}, f32[512]{0:T(512)}, u32[]{:S(2)}) copy-start(f32[512]{0:T(512)} %param.15) | copy-start | bytes 6148
  223.2 2.6 collective-permute-start.3
  224.5 4.8 %collective-permute-start.4 = (bf16[512,8]{0,1:T(8,128)(2,1)S(1)}, bf16[512,8]{0,1:T(8,128)(2,1)S(1)}, u32[]{:S(2)}, u32[]{:S(2)}) collective-permute-start(bf16[512,8]{0,1:T(8,128)(2,1)S(1)} %get-tuple-element.3), channel_id=1, source_target_pairs={{4,0},{8,4},{12,8},{16,12},{20,16},{24,20},{28,24},{5,1},{9,5},{13... | collective-permute-start | bytes 24584 | tf_op jit(solution)/shard_map/ppermute | solution.py:21
  232.7 23.1 %copy-start.5 = (f32[512,2]{0,1:T(2,128)S(1)}, f32[512,2]{0,1:T(2,128)}, u32[]{:S(2)}) copy-start(f32[512,2]{0,1:T(2,128)} %param.23) | copy-start | bytes 12292
  251.2 42.5 %all-to-all-start.1 = ((bf16[8,192,512]{2,1,0:T(8,128)(2,1)}), bf16[8,192,512]{2,1,0:T(8,128)(2,1)}, u32[]{:S(2)}, u32[]{:S(2)}) async-start(bf16[8,192,512]{2,1,0:T(8,128)(2,1)} %bitcast.48), calls=%async_computation.1 | async-start | bytes 3145728 | tf_op jit(solution)/shard_map/all_to_all | solution.py:136
Sparse Core Ops, SparseCore 0:
  68.2 68.8 all-gather.5
  154.4 88.6 all-gather.7
  245.5 35.0 all-gather.3
